TPU v7x, 32 devices: a whole 2x2x4 slice. The times are simulated.
32 devices in a mesh: fs: 8 (over z, y), tp: 4 (over x, core).
Axes of the slice: x: 2, y: 2, z: 4, core: 2. Of those that a mesh axis runs over, the one named last changes fastest.
Arguments:
- tokens: bfloat16 [4096, 2048], P('fs'), may hold values from -6 to 6
- norm_gain: float32 [2048], P('fs'), may hold values from 0.1 to 1.9
- gate_weight: float32 [2048, 6144], P('fs', 'tp'), may hold values from -0.125 to 0.125
- up_weight: float32 [2048, 6144], P('fs', 'tp'), may hold values from -0.125 to 0.125
- down_weight: float32 [6144, 2048], P('fs', 'tp'), may hold values from -0.109375 to 0.109375
Outputs:
- mixed: bfloat16 [4096, 2048], P('fs', 'tp')
- gate_out: bfloat16 [2048, 6144], P(None, 'tp')
- up_out: bfloat16 [2048, 6144], P(None, 'tp')
- down_out: bfloat16 [6144, 2048], P('tp')
All inputs are finite; a program needn't handle non-finite values.
Results may differ from a plain program's by a relative error of at most 0.014.
Values may be sent and summed in bfloat16 or wider, within the bound.
A program may use at most 128 MiB of HBM per device.

v0:
```python
import jax
import jax.numpy as jnp
from jax import lax
from jax.sharding import PartitionSpec as P


def on_device(tokens, norm_gain, gate_weight, up_weight, down_weight):
    row_gain = norm_gain[:, None]
    gate_local = (row_gain * gate_weight).astype(jnp.bfloat16)
    up_local = (row_gain * up_weight).astype(jnp.bfloat16)
    down_local = down_weight.astype(jnp.bfloat16)
    values = tokens.astype(jnp.float32)
    normed = (values * lax.rsqrt(jnp.mean(values * values, axis=1, keepdims=True) + 1e-05)).astype(
        jnp.bfloat16
    )
    w_gate, w_up = (
        lax.all_gather(gate_local, "fs", axis=0, tiled=True),
        lax.all_gather(up_local, "fs", axis=0, tiled=True),
    )
    gate = jnp.dot(normed, w_gate, preferred_element_type=jnp.float32)
    up = jnp.dot(normed, w_up, preferred_element_type=jnp.float32)
    tall_down = lax.all_gather(down_local, "fs", axis=0, tiled=True)
    w_down = lax.all_to_all(tall_down, "tp", split_axis=0, concat_axis=1, tiled=True)
    hidden = (jax.nn.silu(gate) * up).astype(jnp.bfloat16)
    terms = jnp.dot(hidden, w_down, preferred_element_type=jnp.float32).astype(jnp.bfloat16)
    mixed = (
        lax.psum_scatter(terms, "tp", scatter_dimension=1, tiled=True)
        .astype(jnp.float32)
        .astype(jnp.bfloat16)
    )
    return (mixed, w_gate, w_up, w_down)


def solution(mesh):
    return jax.shard_map(
        on_device,
        mesh=mesh,
        in_specs=(P("fs", None), P("fs"), P("fs", "tp"), P("fs", "tp"), P("fs", "tp")),
        out_specs=(P("fs", "tp"), P(None, "tp"), P(None, "tp"), P("tp", None)),
        check_vma=False,
    )
```

profile of v0, /device:TPU:0, one launch (start us, length us, event | category | flops | bytes accessed | tf_op | source)
XLA Modules:
  0.0 373.0 jit_solution(8264817919747729026)
XLA Ops:
  7.2 0.0 all-gather.8.cloned.1.call-start
  7.2 2.5 convert_element_type.28
  9.8 0.0 all-gather.8.cloned.1.call-update
  9.8 0.0 all-gather.4.cloned.1.call-start
  9.9 0.0 copy-done.1
  9.9 1.5 multiply_convert_fusion.1
  11.4 0.0 all-gather.4.cloned.1.call-update
  11.4 0.0 all-gather.6.cloned.1.call-start
  11.5 0.7 all-gather.6.cloned.1.call-update
  12.2 100.0 %all-gather.8.cloned.1.call-done = bf16[6144,512]{1,0:T(8,128)(2,1)} async-done(((bf16[768,512]{1,0:T(8,128)(2,1)}), bf16[6144,512]{1,0:T(8,128)(2,1)}) %all-gather.8.cloned.1.call-update) | async-done | bytes 6291472 | tf_op jit(solution)/shard_map/all_gather | solution.py:22
  112.2 5.4 %all-to-all-start = ((bf16[4,1536,512]{2,1,0:T(8,128)(2,1)}), bf16[4,1536,512]{2,1,0:T(8,128)(2,1)}, u32[]{:S(2)}, u32[]{:S(2)}) async-start(bf16[4,1536,512]{2,1,0:T(8,128)(2,1)} %bitcast.9), calls=%async_computation | async-start | bytes 12582912 | tf_op jit(solution)/shard_map/all_to_all | solution.py:23
  117.6 0.0 reduce-scatter.2.cloned.1.call-start
  117.7 0.5 fusion
  118.2 93.7 %all-gather.4.cloned.1.call-done = bf16[2048,1536]{1,0:T(8,128)(2,1)} async-done(((bf16[256,1536]{1,0:T(8,128)(2,1)}), bf16[2048,1536]{1,0:T(8,128)(2,1)}) %all-gather.4.cloned.1.call-update) | async-done | bytes 6291472 | tf_op jit(solution)/shard_map/all_gather | solution.py:17
  211.9 7.9 %fusion.4 = f32[512,1536]{1,0:T(8,128)} fusion(bf16[2048,1536]{1,0:T(8,128)(2,1)} %all-gather.4.cloned.1.call-done, bf16[512,2048]{1,0:T(8,128)(2,1)S(1)} %copy-done, f32[512]{0:T(512)S(1)} %add_rsqrt_fusion), kind=kOutput, calls=%fused_computation.9 | convolution fusion | flops 3224371200 | bytes 11536384 | tf_op jit(solution)/shard_map/dot_general | solution.py:20
  219.8 0.0 all-to-all-done
  219.8 8.7 %copy.10 = bf16[4,1536,512]{1,2,0:T(8,128)(2,1)} copy(bf16[4,1536,512]{2,1,0:T(8,128)(2,1)} %all-to-all-done) | data formatting | bytes 12582912 | tf_op jit(solution)/shard_map/all_to_all | solution.py:23
  228.5 83.0 %all-gather.6.cloned.1.call-done = bf16[2048,1536]{1,0:T(8,128)(2,1)} async-done(((bf16[256,1536]{1,0:T(8,128)(2,1)}), bf16[2048,1536]{1,0:T(8,128)(2,1)}) %all-gather.6.cloned.1.call-update) | async-done | bytes 6291472 | tf_op jit(solution)/shard_map/all_gather | solution.py:18
  311.5 13.6 %convolution_convert_fusion = bf16[512,2048]{1,0:T(8,128)(2,1)} fusion(bf16[1536,2048]{0,1:T(8,128)(2,1)} %bitcast.7, bf16[2048,1536]{1,0:T(8,128)(2,1)} %all-gather.6.cloned.1.call-done, f32[512,1536]{1,0:T(8,128)} %fusion.4, bf16[512,2048]{1,0:T(8,128)(2,1)S(1)} %copy-done, f32[512]{0:T(512)S(1)} %add_rsqrt_fusion), kind=kOutput, calls=%fused_computation.6 | convolution fusion | flops 6451363840 | bytes 19924992 | tf_op jit(solution)/shard_map/dot_general | solution.py:25
  325.2 0.0 reduce-scatter.2.cloned.1.call-update
  325.2 8.7 %copy.11 = bf16[1536,2048]{1,0:T(8,128)(2,1)} copy(bf16[1536,2048]{0,1:T(8,128)(2,1)} %bitcast.8) | data formatting | bytes 12582912
  333.9 20.8 %reduce-scatter.2.cloned.1.call-done = bf16[512,512]{1,0:T(8,128)(2,1)} async-done(((bf16[512,2048]{1,0:T(8,128)(2,1)}), bf16[512,512]{1,0:T(8,128)(2,1)}) %reduce-scatter.2.cloned.1.call-update) | async-done | bytes 524304 | tf_op jit(solution)/shard_map/reduce_scatter | solution.py:27
  354.7 5.9 %copy.14 = bf16[2048,1536]{1,0:T(8,128)(2,1)} copy(bf16[2048,1536]{1,0:T(8,128)(2,1)} %all-gather.4.cloned.1.call-done) | data formatting | bytes 12582912
  360.6 5.9 %copy.15 = bf16[2048,1536]{1,0:T(8,128)(2,1)} copy(bf16[2048,1536]{1,0:T(8,128)(2,1)} %all-gather.6.cloned.1.call-done) | data formatting | bytes 12582912
  (8 shorter events, 0.0 us)
Async XLA Ops:
  7.2 2.7 copy-start.1
  7.2 2.7 copy-start.3
  7.2 2.7 copy-start.2
  7.2 105.0 %all-gather.8.cloned.1.call-start = ((), (), s32[]{:S(2)}) async-start(), calls=%async_computation.4 | async-start | bytes 7077888 | tf_op jit(solution)/shard_map/all_gather | solution.py:22
  9.8 202.1 %all-gather.4.cloned.1.call-start = ((), (), s32[]{:S(2)}) async-start(), calls=%async_computation.2 | async-start | bytes 7077888 | tf_op jit(solution)/shard_map/all_gather | solution.py:17
  11.4 300.1 %all-gather.6.cloned.1.call-start = ((), (), s32[]{:S(2)}) async-start(), calls=%async_computation.3 | async-start | bytes 7077888 | tf_op jit(solution)/shard_map/all_gather | solution.py:18
  112.2 5.5 %copy-start = (bf16[512,2048]{1,0:T(8,128)(2,1)S(1)}, bf16[512,2048]{1,0:T(8,128)(2,1)}, u32[]{:S(2)}) copy-start(bf16[512,2048]{1,0:T(8,128)(2,1)} %param.5) | copy-start | bytes 6291460
  112.2 107.6 %all-to-all-start = ((bf16[4,1536,512]{2,1,0:T(8,128)(2,1)}), bf16[4,1536,512]{2,1,0:T(8,128)(2,1)}, u32[]{:S(2)}, u32[]{:S(2)}) async-start(bf16[4,1536,512]{2,1,0:T(8,128)(2,1)} %bitcast.9), calls=%async_computation | async-start | bytes 12582912 | tf_op jit(solution)/shard_map/all_to_all | solution.py:23
  117.6 237.1 %reduce-scatter.2.cloned.1.call-start = ((), (), s32[]{:S(2)}) async-start(), calls=%async_computation.5 | async-start | bytes 2621440 | tf_op jit(solution)/shard_map/reduce_scatter | solution.py:27
Sparse Core Ops, SparseCore 0:
  10.8 101.4 all-gather.7
  115.0 96.8 all-gather.3
  214.6 96.8 all-gather.5
  325.3 29.3 reduce-scatter.1
where the time goes:
time: 374 us; the launch traced here: 373 us
  waiting for transfers between devices  298 us (80%)
  local copies, waits for them, and re-layouts  29.2 us (8%)
  matrix products  21.5 us (6%)
  between operations  13.8 us (4%)
  starting transfers between devices  5.56 us (1%)
  other arithmetic  4.56 us (1%)
    all_gather x1, waiting for transfers between devices, on_device(): tall_down = lax.all_gather(down_local, 'fs', axis=0, tiled=True)  100 us
    all_gather x1, waiting for transfers between devices, on_device(): lax.all_gather(gate_local, 'fs', axis=0, tiled=True)  93.7 us
    all_gather x1, waiting for transfers between devices, on_device(): lax.all_gather(up_local, 'fs', axis=0, tiled=True)  83 us
    reduce_scatter x1, waiting for transfers between devices, on_device(): lax.psum_scatter(terms, 'tp', scatter_dimension=1, tiled=True)  20.8 us
    unnamed x11, local copies, waits for them, and re-layouts  20.5 us
    dot_general x1, matrix products, on_device(): jnp.dot(hidden, w_down, preferred_element_type=jnp.float32)  13.6 us
    all_to_all x1, local copies, waits for them, and re-layouts, on_device(): lax.all_to_all(tall_down, 'tp', split_axis=0, concat_axis=1, tiled=True)  8.73 us
    dot_general x1, matrix products, on_device(): gate = jnp.dot(normed, w_gate, preferred_element_type=jnp.float32)  7.9 us
  transfers between devices with their start and end apart: 5, of which 4 were waited for; matrix products, arithmetic and copies ran while one was open for 7% of the time, Pallas kernels for 0%

commit v1 on v0

v1 whole, which is shorter than its diff:
```python
import functools

import jax
import jax.numpy as jnp
from jax import lax
from jax.experimental import pallas as pl
from jax.experimental.pallas import tpu as pltpu
from jax.sharding import PartitionSpec as P

MESH = pl.DeviceIdType.MESH


def lines(fs):
    y = 1
    while 2 * (2 * y) * (2 * y) <= fs:
        y *= 2
    return fs // y, y


def gather_kernel(
    Z, Y, T, nk, nd, detour,
    g_ref, u_ref, d_ref, wg, wu, wd,
    s_up, s_dn, s_y, r_w, s_det, d_up, d_dn, d_y, r_d, s_one, r_one, s_loc,
):
    f, t = lax.axis_index("fs"), lax.axis_index("tp")
    z, y = f // Y, lax.rem(f, Y)
    has_up, has_dn = z < Z - 1, z > 0
    up, dn = (f + Y, t), (f - Y, t)
    others = [lax.rem(y + i, Y) for i in range(1, Y)]
    across = [(z * Y + o, t) for o in others]
    rows = g_ref.shape[0]
    ck = rows // nk
    rows_d, cols_d = d_ref.shape
    cd = rows_d // nd
    own, full = (g_ref, u_ref), (wg, wu)

    def when(cond, fn):
        pl.when(cond)(fn)

    barrier = pltpu.get_barrier_semaphore()

    def greet(dev):
        pl.semaphore_signal(barrier, inc=1, device_id=dev, device_id_type=MESH)

    when(has_up, lambda: greet(up))
    when(has_dn, lambda: greet(dn))
    for dev in across:
        greet(dev)
    for i in range(1, T):
        greet((f, lax.rem(t + i, T)))
    pl.semaphore_wait(barrier, Y + T - 2 + has_up.astype(jnp.int32) + has_dn.astype(jnp.int32))

    def copy(src, dst, ss, rs, dev):
        return pltpu.make_async_remote_copy(
            src_ref=src, dst_ref=dst, send_sem=ss, recv_sem=rs, device_id=dev, device_id_type=MESH
        )

    def part(a, source, k):
        return full[a].at[pl.ds(pl.multiple_of(source * rows + k * ck, ck), ck), :]

    def weight(a, k, source, ss, dev, mine=False):
        src = own[a].at[pl.ds(k * ck, ck), :] if mine else part(a, source, k)
        return copy(src, part(a, source, k), ss, r_w.at[source, a, k], dev)

    def arrived(a, k, source):
        weight(a, k, source, s_det.at[0, a, k], (f, lax.rem(t + 1, T))).wait_recv()

    pieces = [(k, a) for k in range(nk) for a in range(2)]
    sent = []

    def start(cond, make):
        sent.append((cond, make))
        if cond is None:
            make().start()
        else:
            when(cond, lambda: make().start())

    for k, a in pieces:
        start(has_up, lambda k=k, a=a: weight(a, k, f, s_up.at[z, a, k], up, True))
        start(has_dn, lambda k=k, a=a: weight(a, k, f, s_dn.at[z, a, k], dn, True))
        for i in range(Y - 1):
            start(None, lambda k=k, a=a, i=i: weight(a, k, f, s_y.at[i, z, a, k], across[i], True))

    def column(owner):
        return wd.at[
            pl.ds(pl.multiple_of(y * rows_d, rows_d), rows_d),
            pl.ds(pl.multiple_of(owner * cols_d, cols_d), cols_d),
        ]

    def first(owner, dev):
        return copy(d_ref, column(owner), s_one.at[0], r_one.at[owner], dev)

    start(z != t, lambda: first(t, (f, z)))

    locals_ = [
        pltpu.make_async_copy(
            own[a], full[a].at[pl.ds(pl.multiple_of(f * rows, rows), rows), :], s_loc.at[a]
        )
        for a in range(2)
    ]
    for c in locals_:
        c.start()
    keep = pltpu.make_async_copy(d_ref, column(t), s_loc.at[2])
    when(z == t, lambda: keep.start())

    for k, a in pieces:
        if k >= detour:
            continue
        source = across[0][0]
        arrived(a, k, source)
        start(has_up, lambda k=k, a=a, s=source: weight(a, k, s, s_det.at[0, a, k], up))
        start(has_dn, lambda k=k, a=a, s=source: weight(a, k, s, s_det.at[1, a, k], dn))

    for step in range(1, Z):
        for k, a in pieces:
            for sign in (-1, 1):
                zs = z + sign * step
                source = zs * Y + y
                valid = zs >= 0 if sign < 0 else zs < Z
                onward = jnp.logical_and(valid, has_up if sign < 0 else has_dn)
                when(valid, lambda a=a, k=k, s=source: arrived(a, k, s))
                if sign < 0:
                    start(onward, lambda a=a, k=k, s=source, q=zs: weight(a, k, s, s_up.at[q, a, k], up))
                else:
                    start(onward, lambda a=a, k=k, s=source, q=zs: weight(a, k, s, s_dn.at[q, a, k], dn))
                if step == 1 and k < detour:
                    continue
                for i in range(Y - 1):
                    start(valid, lambda a=a, k=k, s=source, q=zs, i=i: weight(a, k, s, s_y.at[i, q, a, k], across[i]))

    def rows_of(line, k):
        return wd.at[pl.ds(pl.multiple_of(line * rows_d + k * cd, cd), cd), :]

    def down(k, ss, dev, line):
        return copy(rows_of(line, k), rows_of(line, k), ss, r_d.at[line, k], dev)

    def down_arrived(k, line):
        down(k, d_up.at[k], (f, lax.rem(t + 1, T)), line).wait_recv()

    def assemble():
        keep.wait()
        for i in range(1, T):
            owner = lax.rem(t + i, T)
            first(owner, (f, owner)).wait_recv()

    when(z == t, assemble)
    go_up = jnp.logical_and(z >= t, has_up)
    go_dn = jnp.logical_and(z <= t, has_dn)
    for k in range(nd):
        when(z != t, lambda k=k: down_arrived(k, y))
        start(go_up, lambda k=k: down(k, d_up.at[k], up, y))
        start(go_dn, lambda k=k: down(k, d_dn.at[k], dn, y))
        for i in range(Y - 1):
            start(None, lambda k=k, i=i: down(k, d_y.at[i, k], across[i], y))

    for zs in range(Z):
        for o in others:
            for k, a in pieces:
                if k < detour:
                    when(zs != z, lambda a=a, k=k, zs=zs, o=o: arrived(a, k, zs * Y + o))
                else:
                    arrived(a, k, zs * Y + o)
    for o in others:
        for k in range(nd):
            down_arrived(k, o)
    for c in locals_:
        c.wait()
    for cond, make in sent:
        if cond is None:
            make().wait_send()
        else:
            when(cond, lambda make=make: make().wait_send())


def gather(mesh, g, u, d):
    fs, T = mesh.shape["fs"], mesh.shape["tp"]
    Z, Y = lines(fs)
    rows, rows_d = g.shape[0], d.shape[0]
    nk = max(1, min(4, rows // 64))
    nd = max(1, min(8, rows_d // 96))
    detour = nk // 2 if Y == 2 else 0
    dma = pltpu.SemaphoreType.DMA
    any_ = pl.BlockSpec(memory_space=pl.ANY)
    return pl.pallas_call(
        functools.partial(gather_kernel, Z, Y, T, nk, nd, detour),
        out_shape=(
            jax.ShapeDtypeStruct((rows * fs, g.shape[1]), g.dtype),
            jax.ShapeDtypeStruct((rows * fs, g.shape[1]), g.dtype),
            jax.ShapeDtypeStruct((rows_d * Y, d.shape[1] * T), d.dtype),
        ),
        in_specs=[any_] * 3,
        out_specs=[any_] * 3,
        scratch_shapes=[
            dma((Z, 2, nk)), dma((Z, 2, nk)), dma((max(Y - 1, 1), Z, 2, nk)), dma((fs, 2, nk)),
            dma((2, 2, nk)), dma((nd,)), dma((nd,)), dma((max(Y - 1, 1), nd)), dma((Y, nd)),
            dma((1,)), dma((T,)), dma((3,)),
        ],
        compiler_params=pltpu.CompilerParams(collective_id=0, has_side_effects=True),
        name="gather",
    )(g, u, d)


def layer_kernel(x_ref, wg, wu, wd, part, og, ou, od, normed, total):
    j = pl.program_id(0)

    @pl.when(j == 0)
    def _():
        v = x_ref[...].astype(jnp.float32)
        normed[...] = (v * lax.rsqrt(jnp.mean(v * v, axis=1, keepdims=True) + 1e-05)).astype(jnp.bfloat16)
        total[...] = jnp.zeros_like(total)

    og[...] = wg[...]
    ou[...] = wu[...]
    od[...] = wd[...]
    gate = jnp.dot(normed[...], wg[...], preferred_element_type=jnp.float32)
    up = jnp.dot(normed[...], wu[...], preferred_element_type=jnp.float32)
    hidden = (gate / (1.0 + jnp.exp(-gate)) * up).astype(jnp.bfloat16)
    total[...] += jnp.dot(hidden, wd[...], preferred_element_type=jnp.float32)

    @pl.when(j == pl.num_programs(0) - 1)
    def _():
        part[...] = total[...].astype(jnp.bfloat16)


def layer(x, wg, wu, wd):
    n, depth = x.shape
    units = wg.shape[1]
    width = 256 if units % 256 == 0 else 128
    spec_w = pl.BlockSpec((depth, width), lambda j: (0, j))
    spec_d = pl.BlockSpec((width, wd.shape[1]), lambda j: (j, 0))
    whole = pl.BlockSpec((n, depth), lambda j: (0, 0))
    return pl.pallas_call(
        layer_kernel,
        grid=(units // width,),
        out_shape=(
            jax.ShapeDtypeStruct((n, wd.shape[1]), jnp.bfloat16),
            jax.ShapeDtypeStruct(wg.shape, wg.dtype),
            jax.ShapeDtypeStruct(wu.shape, wu.dtype),
            jax.ShapeDtypeStruct(wd.shape, wd.dtype),
        ),
        in_specs=[whole, spec_w, spec_w, spec_d],
        out_specs=[pl.BlockSpec((n, wd.shape[1]), lambda j: (0, 0)), spec_w, spec_w, spec_d],
        scratch_shapes=[
            pltpu.VMEM((n, depth), jnp.bfloat16),
            pltpu.VMEM((n, wd.shape[1]), jnp.float32),
        ],
        compiler_params=pltpu.CompilerParams(vmem_limit_bytes=60 * 1024 * 1024),
        name="layer",
    )(x, wg, wu, wd)


def sum_kernel(X, nc, p_ref, o_ref, near, pair, far, s_a, r_a, s_b, r_b):
    f, t = lax.axis_index("fs"), lax.axis_index("tp")
    x, core = t // 2, lax.rem(t, 2)
    mate = (f, x * 2 + 1 - core)
    n, width = o_ref.shape
    h = n // nc
    barrier = pltpu.get_barrier_semaphore()
    xs = [lax.rem(x + i, X) for i in range(1, X)]
    peers = [mate] + [(f, q * 2 + core) for q in xs]
    for dev in peers:
        pl.semaphore_signal(barrier, inc=1, device_id=dev, device_id_type=MESH)
    pl.semaphore_wait(barrier, len(peers))

    order = [(c, i) for c in range(nc) for i in list(range(1, X)) + [0]]

    def block(c, i, which):
        q = lax.rem(x + i, X)
        start = pl.multiple_of((q * 2 + which) * width, width)
        return p_ref.at[pl.ds(c * h, h), pl.ds(start, width)]

    def to_mate(c, i):
        return pltpu.make_async_remote_copy(
            src_ref=block(c, i, 1 - core), dst_ref=near.at[i, pl.ds(c * h, h), :],
            send_sem=s_a.at[i, c], recv_sem=r_a.at[i, c], device_id=mate, device_id_type=MESH,
        )

    def to_far(c, i):
        return pltpu.make_async_remote_copy(
            src_ref=pair.at[i, pl.ds(c * h, h), :], dst_ref=far.at[i, pl.ds(c * h, h), :],
            send_sem=s_b.at[i, c], recv_sem=r_b.at[i, c], device_id=peers[i], device_id_type=MESH,
        )

    order = [(c, i) for c in range(nc) for i in range(1, X)]
    for c, i in order:
        to_mate(c, i).start()
    for c in range(nc):
        to_mate(c, 0).start()
    for c, i in order:
        to_mate(c, i).wait_recv()
        pair[i, pl.ds(c * h, h), :] = (
            block(c, i, core)[...].astype(jnp.float32) + near[i, pl.ds(c * h, h), :].astype(jnp.float32)
        ).astype(jnp.bfloat16)
        to_far(c, i).start()
    for c in range(nc):
        to_mate(c, 0).wait_recv()
        acc = block(c, 0, core)[...].astype(jnp.float32) + near[0, pl.ds(c * h, h), :].astype(jnp.float32)
        for i in range(1, X):
            to_far(c, i).wait_recv()
            acc = acc + far[i, pl.ds(c * h, h), :].astype(jnp.float32)
        o_ref[pl.ds(c * h, h), :] = acc.astype(o_ref.dtype)
    for c in range(nc):
        for i in range(X):
            to_mate(c, i).wait_send()
            if i:
                to_far(c, i).wait_send()


def sum_parts(mesh, p):
    T = mesh.shape["tp"]
    X = T // 2
    n, width = p.shape[0], p.shape[1] // T
    nc = 4
    dma = pltpu.SemaphoreType.DMA
    vmem = pl.BlockSpec(memory_space=pltpu.VMEM)
    return pl.pallas_call(
        functools.partial(sum_kernel, X, nc),
        out_shape=jax.ShapeDtypeStruct((n, width), jnp.bfloat16),
        in_specs=[vmem],
        out_specs=vmem,
        scratch_shapes=[pltpu.VMEM((X, n, width), jnp.bfloat16)] * 3 + [dma((X, nc))] * 4,
        compiler_params=pltpu.CompilerParams(
            collective_id=1, has_side_effects=True, vmem_limit_bytes=48 * 1024 * 1024
        ),
        name="sum_parts",
    )(p)


def solution(mesh):
    def on_device(tokens, norm_gain, gate_weight, up_weight, down_weight):
        row_gain = norm_gain[:, None]
        gate_local = (row_gain * gate_weight).astype(jnp.bfloat16)
        up_local = (row_gain * up_weight).astype(jnp.bfloat16)
        down_local = down_weight.astype(jnp.bfloat16)
        wg, wu, wd = gather(mesh, gate_local, up_local, down_local)
        part, og, ou, od = layer(tokens, wg, wu, wd)
        return (sum_parts(mesh, part), og, ou, od)

    return jax.shard_map(
        on_device,
        mesh=mesh,
        in_specs=(P("fs", None), P("fs"), P("fs", "tp"), P("fs", "tp"), P("fs", "tp")),
        out_specs=(P("fs", "tp"), P(None, "tp"), P(None, "tp"), P("tp", None)),
        check_vma=False,
    )
```

time: 374 us -> 248 us (0.66)
  waiting for transfers between devices: 298 us -> 0 us
  Pallas kernels: 0 us -> 239 us
  local copies, waits for them, and re-layouts: 29.2 us -> 2.39 us
  matrix products: 21.5 us -> 0 us
  between operations: 13.8 us -> 0.67 us
  starting transfers between devices: 5.56 us -> 0 us
    all_gather x3 -> x0, waiting for transfers between devices: 277 us -> none  [the longest x1 100 us: on_device(): tall_down = lax.all_gather(down_local, 'fs', axis=0, tiled=True)]
    pallas_call x0 -> x3, Pallas kernels: none -> 239 us  [the longest x1 199 us: gather(): pl.pallas_call(functools.partial(gather_kernel, Z, Y, T, nk, nd, detour),...]
    dot_general x2 -> x0, matrix products: 21.5 us -> none  [the longest x1 13.6 us: on_device(): jnp.dot(hidden, w_down, preferred_element_type=jnp.float32)]
    reduce_scatter x1 -> x0, waiting for transfers between devices: 20.8 us -> none  [on_device(): lax.psum_scatter(terms, 'tp', scatter_dimension=1, tiled=True)]
    unnamed x11 -> x7, local copies, waits for them, and re-layouts: 20.5 us -> 2.39 us
    all_to_all x1 -> x0, local copies, waits for them, and re-layouts: 8.73 us -> none  [on_device(): lax.all_to_all(tall_down, 'tp', split_axis=0, concat_axis=1, tiled=True)]
    all_to_all x1 -> x0, starting transfers between devices: 5.4 us -> none  [on_device(): lax.all_to_all(tall_down, 'tp', split_axis=0, concat_axis=1, tiled=True)]
  transfers between devices with their start and end apart: 5 -> 0, of which waited for: 4 -> 0; matrix products, arithmetic and copies ran while one was open for 7% -> 0% of each run, Pallas kernels for 0% -> 0%
where the time goes in v1:
time: 248 us
  Pallas kernels  239 us (96%)
  other arithmetic  5.46 us (2%)
    pallas_call x1, Pallas kernels, gather(): pl.pallas_call(functools.partial(gather_kernel, Z, Y, T, nk, nd, detour),...  199 us
    pallas_call x1, Pallas kernels, layer(): pl.pallas_call(layer_kernel, grid=(units // width,), out_shape=(jax.Shape...  21.2 us
    pallas_call x1, Pallas kernels, sum_parts(): pl.pallas_call(functools.partial(sum_kernel, X, nc), out_shape=jax.ShapeD...  18.7 us

profile of v1, /device:TPU:0, one launch (start us, length us, event | category | flops | bytes accessed | tf_op | source)
XLA Modules:
  0.0 247.6 jit_solution(16771402318260478120)
XLA Ops:
  0.6 0.0 copy-start.1
  0.6 0.0 copy-start.2
  0.7 2.5 %convert_element_type.11.d_ref = bf16[768,512]{1,0:T(8,128)(2,1)} convert(f32[768,512]{1,0:T(8,128)} %param.9) | non-fusion elementwise | flops 393216 | bytes 2359296 | tf_op jit(solution)/shard_map/convert_element_type | solution.py:334
  3.2 0.0 copy-done.1
  3.2 0.0 copy-done.2
  3.2 3.0 %multiply_convert_fusion = (bf16[256,1536]{1,0:T(8,128)(2,1)}, bf16[256,1536]{1,0:T(8,128)(2,1)}) fusion(f32[256,1536]{1,0:T(8,128)S(1)} %copy-done.1, f32[256]{0:T(256)S(1)} %copy-done.2, f32[256,1536]{1,0:T(8,128)} %param.7), kind=kLoop, calls=%fused_computation | loop fusion | flops 1572864 | bytes 4719616 | tf_op jit(solution)/shard_map/convert_element_type | solution.py:333
  6.1 199.1 %gather.1 = (bf16[2048,1536]{1,0:T(8,128)(2,1)}, bf16[2048,1536]{1,0:T(8,128)(2,1)}, bf16[1536,2048]{1,0:T(8,128)(2,1)}) custom-call(bf16[256,1536]{1,0:T(8,128)(2,1)} %get-tuple-element.19.g_ref, bf16[256,1536]{1,0:T(8,128)(2,1)} %get-tuple-element.18.u_ref, bf16[768,512]{1,0:T(8,128)(2,1)} %convert_element_type.11.d_ref), custom_call_target="tpu_custom_call" | custom-call | tf_op jit(solution)/shard_map/gather/pallas_call | solution.py:184
  205.2 21.2 %layer.1 = (bf16[512,2048]{1,0:T(8,128)(2,1)}, bf16[2048,1536]{1,0:T(8,128)(2,1)}, bf16[2048,1536]{1,0:T(8,128)(2,1)}, bf16[1536,2048]{1,0:T(8,128)(2,1)}) custom-call(bf16[512,2048]{1,0:T(8,128)(2,1)} %x_ref.1, bf16[2048,1536]{1,0:T(8,128)(2,1)} %get-tuple-element.11.wg, bf16[2048,1536]{1,0:T(8,128)(2,1)} %get-tuple-element.12.wu, ...), custom_call_target="tpu_custom_call" | custom-call | tf_op jit(solution)/shard_map/layer/pallas_call | solution.py:232
  226.5 0.0 copy-start
  226.5 1.6 copy-done
  228.1 18.7 %sum_parts.1 = bf16[512,512]{1,0:T(8,128)(2,1)S(1)} custom-call(bf16[512,2048]{1,0:T(8,128)(2,1)S(1)} %copy-done), custom_call_target="tpu_custom_call" | custom-call | tf_op jit(solution)/shard_map/sum_parts/pallas_call | solution.py:316
  246.8 0.8 copy.10
Async XLA Ops:
  0.6 2.5 %copy-start.1 = (f32[256,1536]{1,0:T(8,128)S(1)}, f32[256,1536]{1,0:T(8,128)}, u32[]{:S(2)}) copy-start(f32[256,1536]{1,0:T(8,128)} %param.8) | copy-start | bytes 4718596
  0.6 2.5 %copy-start.2 = (f32[256]{0:T(256)S(1)}, f32[256]{0:T(256)}, u32[]{:S(2)}) copy-start(f32[256]{0:T(256)} %param.6) | copy-start | bytes 3076
  226.5 1.6 copy-start

commit v2 on v1

--- a/solution.py
+++ b/solution.py
@@ -8,6 +8,7 @@
 from jax.sharding import PartitionSpec as P
 
 MESH = pl.DeviceIdType.MESH
+GRANT = 16 * 1024 * 1024
 
 
 def lines(fs):
@@ -19,8 +20,8 @@
 
 def gather_kernel(
     Z, Y, T, nk, nd, detour,
-    g_ref, u_ref, d_ref, wg, wu, wd,
-    s_up, s_dn, s_y, r_w, s_det, d_up, d_dn, d_y, r_d, s_one, r_one, s_loc,
+    g_ref, u_ref, d_ref, x_ref, wg, wu, wd, hidden,
+    normed, s_up, s_dn, s_y, r_w, s_det, d_up, d_dn, d_y, r_d, s_one, r_one,
 ):
     f, t = lax.axis_index("fs"), lax.axis_index("tp")
     z, y = f // Y, lax.rem(f, Y)
@@ -92,16 +93,25 @@
 
     start(z != t, lambda: first(t, (f, z)))
 
-    locals_ = [
-        pltpu.make_async_copy(
-            own[a], full[a].at[pl.ds(pl.multiple_of(f * rows, rows), rows), :], s_loc.at[a]
-        )
-        for a in range(2)
-    ]
-    for c in locals_:
-        c.start()
-    keep = pltpu.make_async_copy(d_ref, column(t), s_loc.at[2])
-    when(z == t, lambda: keep.start())
+    for a in range(2):
+        full[a][pl.ds(pl.multiple_of(f * rows, rows), rows), :] = own[a][...]
+
+    def keep():
+        wd[
+            pl.ds(pl.multiple_of(y * rows_d, rows_d), rows_d),
+            pl.ds(pl.multiple_of(t * cols_d, cols_d), cols_d),
+        ] = d_ref[...]
+
+    when(z == t, keep)
+
+    n = x_ref.shape[0]
+    slab = 64 if n % 64 == 0 else n
+
+    @pl.loop(0, n // slab)
+    def _(i):
+        at = pl.ds(pl.multiple_of(i * slab, slab), slab)
+        v = x_ref[at, :].astype(jnp.float32)
+        normed[at, :] = (v * lax.rsqrt(jnp.mean(v * v, axis=1, keepdims=True) + 1e-05)).astype(jnp.bfloat16)
 
     for k, a in pieces:
         if k >= detour:
@@ -138,7 +148,6 @@
         down(k, d_up.at[k], (f, lax.rem(t + 1, T)), line).wait_recv()
 
     def assemble():
-        keep.wait()
         for i in range(1, T):
             owner = lax.rem(t + i, T)
             first(owner, (f, owner)).wait_recv()
@@ -160,11 +169,19 @@
                     when(zs != z, lambda a=a, k=k, zs=zs, o=o: arrived(a, k, zs * Y + o))
                 else:
                     arrived(a, k, zs * Y + o)
+    units = wg.shape[1]
+    width = 256 if units % 256 == 0 else 128
+
+    @pl.loop(0, units // width)
+    def _(j):
+        at = pl.ds(pl.multiple_of(j * width, width), width)
+        gate = jnp.dot(normed[...], wg[:, at], preferred_element_type=jnp.float32)
+        up_ = jnp.dot(normed[...], wu[:, at], preferred_element_type=jnp.float32)
+        hidden[:, at] = (gate / (1.0 + jnp.exp(-gate)) * up_).astype(jnp.bfloat16)
+
     for o in others:
         for k in range(nd):
             down_arrived(k, o)
-    for c in locals_:
-        c.wait()
     for cond, make in sent:
         if cond is None:
             make().wait_send()
@@ -172,7 +189,7 @@
             when(cond, lambda make=make: make().wait_send())
 
 
-def gather(mesh, g, u, d):
+def gather(mesh, g, u, d, x):
     fs, T = mesh.shape["fs"], mesh.shape["tp"]
     Z, Y = lines(fs)
     rows, rows_d = g.shape[0], d.shape[0]
@@ -180,73 +197,61 @@
     nd = max(1, min(8, rows_d // 96))
     detour = nk // 2 if Y == 2 else 0
     dma = pltpu.SemaphoreType.DMA
-    any_ = pl.BlockSpec(memory_space=pl.ANY)
+    vmem = pl.BlockSpec(memory_space=pltpu.VMEM)
     return pl.pallas_call(
         functools.partial(gather_kernel, Z, Y, T, nk, nd, detour),
         out_shape=(
             jax.ShapeDtypeStruct((rows * fs, g.shape[1]), g.dtype),
             jax.ShapeDtypeStruct((rows * fs, g.shape[1]), g.dtype),
             jax.ShapeDtypeStruct((rows_d * Y, d.shape[1] * T), d.dtype),
+            jax.ShapeDtypeStruct((x.shape[0], g.shape[1]), d.dtype),
         ),
-        in_specs=[any_] * 3,
-        out_specs=[any_] * 3,
+        in_specs=[vmem] * 4,
+        out_specs=[vmem] * 4,
         scratch_shapes=[
+            pltpu.VMEM(x.shape, x.dtype),
             dma((Z, 2, nk)), dma((Z, 2, nk)), dma((max(Y - 1, 1), Z, 2, nk)), dma((fs, 2, nk)),
             dma((2, 2, nk)), dma((nd,)), dma((nd,)), dma((max(Y - 1, 1), nd)), dma((Y, nd)),
-            dma((1,)), dma((T,)), dma((3,)),
+            dma((1,)), dma((T,)),
         ],
-        compiler_params=pltpu.CompilerParams(collective_id=0, has_side_effects=True),
+        compiler_params=pltpu.CompilerParams(
+            collective_id=0, has_side_effects=True, vmem_limit_bytes=GRANT
+        ),
         name="gather",
-    )(g, u, d)
-
-
-def layer_kernel(x_ref, wg, wu, wd, part, og, ou, od, normed, total):
-    j = pl.program_id(0)
-
-    @pl.when(j == 0)
-    def _():
-        v = x_ref[...].astype(jnp.float32)
-        normed[...] = (v * lax.rsqrt(jnp.mean(v * v, axis=1, keepdims=True) + 1e-05)).astype(jnp.bfloat16)
-        total[...] = jnp.zeros_like(total)
-
-    og[...] = wg[...]
-    ou[...] = wu[...]
-    od[...] = wd[...]
-    gate = jnp.dot(normed[...], wg[...], preferred_element_type=jnp.float32)
-    up = jnp.dot(normed[...], wu[...], preferred_element_type=jnp.float32)
-    hidden = (gate / (1.0 + jnp.exp(-gate)) * up).astype(jnp.bfloat16)
-    total[...] += jnp.dot(hidden, wd[...], preferred_element_type=jnp.float32)
-
-    @pl.when(j == pl.num_programs(0) - 1)
-    def _():
-        part[...] = total[...].astype(jnp.bfloat16)
-
-
-def layer(x, wg, wu, wd):
-    n, depth = x.shape
-    units = wg.shape[1]
-    width = 256 if units % 256 == 0 else 128
-    spec_w = pl.BlockSpec((depth, width), lambda j: (0, j))
-    spec_d = pl.BlockSpec((width, wd.shape[1]), lambda j: (j, 0))
-    whole = pl.BlockSpec((n, depth), lambda j: (0, 0))
+    )(g, u, d, x)
+
+
+def layer_kernel(T, h_ref, wg, wu, wd, part, og, ou, od, sems):
+    outs = [pltpu.make_async_copy(s, d, sems.at[i]) for i, (s, d) in enumerate(((wg, og), (wu, ou), (wd, od)))]
+    for c in outs:
+        c.start()
+    width = part.shape[1] // T
+
+    @pl.loop(0, T)
+    def _(j):
+        at = pl.ds(pl.multiple_of(j * width, width), width)
+        part[:, at] = jnp.dot(h_ref[...], wd[:, at], preferred_element_type=jnp.float32).astype(jnp.bfloat16)
+
+    for c in outs:
+        c.wait()
+
+
+def layer(mesh, h, wg, wu, wd):
+    vmem, any_ = pl.BlockSpec(memory_space=pltpu.VMEM), pl.BlockSpec(memory_space=pl.ANY)
     return pl.pallas_call(
-        layer_kernel,
-        grid=(units // width,),
+        functools.partial(layer_kernel, mesh.shape["tp"]),
         out_shape=(
-            jax.ShapeDtypeStruct((n, wd.shape[1]), jnp.bfloat16),
+            jax.ShapeDtypeStruct((h.shape[0], wd.shape[1]), jnp.bfloat16),
             jax.ShapeDtypeStruct(wg.shape, wg.dtype),
             jax.ShapeDtypeStruct(wu.shape, wu.dtype),
             jax.ShapeDtypeStruct(wd.shape, wd.dtype),
         ),
-        in_specs=[whole, spec_w, spec_w, spec_d],
-        out_specs=[pl.BlockSpec((n, wd.shape[1]), lambda j: (0, 0)), spec_w, spec_w, spec_d],
-        scratch_shapes=[
-            pltpu.VMEM((n, depth), jnp.bfloat16),
-            pltpu.VMEM((n, wd.shape[1]), jnp.float32),
-        ],
-        compiler_params=pltpu.CompilerParams(vmem_limit_bytes=60 * 1024 * 1024),
+        in_specs=[vmem] * 4,
+        out_specs=[vmem] + [any_] * 3,
+        scratch_shapes=[pltpu.SemaphoreType.DMA((3,))],
+        compiler_params=pltpu.CompilerParams(vmem_limit_bytes=GRANT),
         name="layer",
-    )(x, wg, wu, wd)
+    )(h, wg, wu, wd)
 
 
 def sum_kernel(X, nc, p_ref, o_ref, near, pair, far, s_a, r_a, s_b, r_b):
@@ -320,7 +325,7 @@
         out_specs=vmem,
         scratch_shapes=[pltpu.VMEM((X, n, width), jnp.bfloat16)] * 3 + [dma((X, nc))] * 4,
         compiler_params=pltpu.CompilerParams(
-            collective_id=1, has_side_effects=True, vmem_limit_bytes=48 * 1024 * 1024
+            collective_id=1, has_side_effects=True, vmem_limit_bytes=16 * 1024 * 1024
         ),
         name="sum_parts",
     )(p)
@@ -332,8 +337,8 @@
         gate_local = (row_gain * gate_weight).astype(jnp.bfloat16)
         up_local = (row_gain * up_weight).astype(jnp.bfloat16)
         down_local = down_weight.astype(jnp.bfloat16)
-        wg, wu, wd = gather(mesh, gate_local, up_local, down_local)
-        part, og, ou, od = layer(tokens, wg, wu, wd)
+        wg, wu, wd, hidden = gather(mesh, gate_local, up_local, down_local, tokens)
+        part, og, ou, od = layer(mesh, hidden, wg, wu, wd)
         return (sum_parts(mesh, part), og, ou, od)
 
     return jax.shard_map(

time: 248 us -> 230 us (0.927)
  Pallas kernels: 239 us -> 225 us
    pallas_call x1, Pallas kernels: 21.2 us -> 6.69 us  [layer(): pl.pallas_call(functools.partial(layer_kernel, mesh.shape['tp']), out_sha...]
where the time goes in v2:
time: 230 us
  Pallas kernels  225 us (98%)
  other arithmetic  3.59 us (2%)
    pallas_call x1, Pallas kernels, gather(): pl.pallas_call(functools.partial(gather_kernel, Z, Y, T, nk, nd, detour),...  198 us
    pallas_call x1, Pallas kernels, sum_parts(): pl.pallas_call(functools.partial(sum_kernel, X, nc), out_shape=jax.ShapeD...  19.6 us
    pallas_call x1, Pallas kernels, layer(): pl.pallas_call(functools.partial(layer_kernel, mesh.shape['tp']), out_sha...  6.69 us

profile of v2, /device:TPU:0, one launch (start us, length us, event | category | flops | bytes accessed | tf_op | source)
XLA Modules:
  0.0 230.1 jit_solution(4663961349328801851)
XLA Ops:
  0.6 0.0 copy-start.1
  0.6 0.0 copy-start.2
  0.7 1.6 convert_element_type.11.d_ref
  2.3 0.2 copy-done.1
  2.5 0.0 copy-done.2
  2.5 0.0 copy-start
  2.5 2.0 multiply_convert_fusion
  4.5 0.1 copy-done
  4.6 198.4 %gather.1 = (bf16[2048,1536]{1,0:T(8,128)(2,1)S(1)}, bf16[2048,1536]{1,0:T(8,128)(2,1)S(1)}, bf16[1536,2048]{1,0:T(8,128)(2,1)S(1)}, bf16[512,1536]{1,0:T(8,128)(2,1)S(1)}) custom-call(bf16[256,1536]{1,0:T(8,128)(2,1)S(1)} %get-tuple-element.21.g_ref, bf16[256,1536]{1,0:T(8,128)(2,1)S(1)} %get-tuple-element.20.u_ref, ...), custom_call_target="tpu_custom_call" | custom-call | tf_op jit(solution)/shard_map/gather/pallas_call | solution.py:201
  203.0 6.7 %layer.1 = (bf16[512,2048]{1,0:T(8,128)(2,1)S(1)}, bf16[2048,1536]{1,0:T(8,128)(2,1)}, bf16[2048,1536]{1,0:T(8,128)(2,1)}, bf16[1536,2048]{1,0:T(8,128)(2,1)}) custom-call(bf16[512,1536]{1,0:T(8,128)(2,1)S(1)} %get-tuple-element.12.h_ref, bf16[2048,1536]{1,0:T(8,128)(2,1)S(1)} %get-tuple-element.13.wg, bf16[2048,1536]{1,0:T(8,128)(2,1)S(1)} %get-tuple-element.14.wu, ...), custom_call_target="tpu_custom_call" | custom-call | tf_op jit(solution)/shard_map/layer/pallas_call | solution.py:241
  209.7 19.6 %sum_parts.1 = bf16[512,512]{1,0:T(8,128)(2,1)S(1)} custom-call(bf16[512,2048]{1,0:T(8,128)(2,1)S(1)} %get-tuple-element.16.p_ref), custom_call_target="tpu_custom_call" | custom-call | tf_op jit(solution)/shard_map/sum_parts/pallas_call | solution.py:321
  229.3 0.8 copy.10
Async XLA Ops:
  0.6 1.9 copy-start.1
  0.6 1.9 copy-start.2
  2.5 2.1 copy-start

commit v3 on v2

--- a/solution.py
+++ b/solution.py
@@ -194,7 +194,7 @@
     Z, Y = lines(fs)
     rows, rows_d = g.shape[0], d.shape[0]
     nk = max(1, min(4, rows // 64))
-    nd = max(1, min(8, rows_d // 96))
+    nd = max(1, min(16, rows_d // 48))
     detour = nk // 2 if Y == 2 else 0
     dma = pltpu.SemaphoreType.DMA
     vmem = pl.BlockSpec(memory_space=pltpu.VMEM)

time: 230 us -> 228 us (level)
    pallas_call x1, Pallas kernels: 19.6 us -> 16.4 us  [sum_parts(): pl.pallas_call(functools.partial(sum_kernel, X, nc), out_shape=jax.ShapeD...]
where the time goes in v3:
time: 228 us
  Pallas kernels  223 us (98%)
  other arithmetic  3.59 us (2%)
    pallas_call x1, Pallas kernels, gather(): pl.pallas_call(functools.partial(gather_kernel, Z, Y, T, nk, nd, detour),...  199 us
    pallas_call x1, Pallas kernels, sum_parts(): pl.pallas_call(functools.partial(sum_kernel, X, nc), out_shape=jax.ShapeD...  16.4 us
    pallas_call x1, Pallas kernels, layer(): pl.pallas_call(functools.partial(layer_kernel, mesh.shape['tp']), out_sha...  6.69 us

profile of v3, /device:TPU:0, one launch (start us, length us, event | category | flops | bytes accessed | tf_op | source)
XLA Modules:
  0.0 228.0 jit_solution(4000525347265651649)
XLA Ops:
  0.6 0.0 copy-start.1
  0.6 0.0 copy-start.2
  0.7 1.6 convert_element_type.11.d_ref
  2.3 0.2 copy-done.1
  2.5 0.0 copy-done.2
  2.5 0.0 copy-start
  2.5 2.0 multiply_convert_fusion
  4.5 0.1 copy-done
  4.6 199.5 %gather.1 = (bf16[2048,1536]{1,0:T(8,128)(2,1)S(1)}, bf16[2048,1536]{1,0:T(8,128)(2,1)S(1)}, bf16[1536,2048]{1,0:T(8,128)(2,1)S(1)}, bf16[512,1536]{1,0:T(8,128)(2,1)S(1)}) custom-call(bf16[256,1536]{1,0:T(8,128)(2,1)S(1)} %get-tuple-element.21.g_ref, bf16[256,1536]{1,0:T(8,128)(2,1)S(1)} %get-tuple-element.20.u_ref, ...), custom_call_target="tpu_custom_call" | custom-call | tf_op jit(solution)/shard_map/gather/pallas_call | solution.py:201
  204.0 6.7 %layer.1 = (bf16[512,2048]{1,0:T(8,128)(2,1)S(1)}, bf16[2048,1536]{1,0:T(8,128)(2,1)}, bf16[2048,1536]{1,0:T(8,128)(2,1)}, bf16[1536,2048]{1,0:T(8,128)(2,1)}) custom-call(bf16[512,1536]{1,0:T(8,128)(2,1)S(1)} %get-tuple-element.12.h_ref, bf16[2048,1536]{1,0:T(8,128)(2,1)S(1)} %get-tuple-element.13.wg, bf16[2048,1536]{1,0:T(8,128)(2,1)S(1)} %get-tuple-element.14.wu, ...), custom_call_target="tpu_custom_call" | custom-call | tf_op jit(solution)/shard_map/layer/pallas_call | solution.py:241
  210.7 16.4 %sum_parts.1 = bf16[512,512]{1,0:T(8,128)(2,1)S(1)} custom-call(bf16[512,2048]{1,0:T(8,128)(2,1)S(1)} %get-tuple-element.16.p_ref), custom_call_target="tpu_custom_call" | custom-call | tf_op jit(solution)/shard_map/sum_parts/pallas_call | solution.py:321
  227.2 0.8 copy.10
Async XLA Ops:
  0.6 1.9 copy-start.1
  0.6 1.9 copy-start.2
  2.5 2.1 copy-start
